TPU v7x, 256 devices: a whole 4x4x8 slice. The times are simulated.
256 devices in a mesh: sp: 16 (over y, x), tp: 16 (over z, core).
Axes of the slice: x: 4, y: 4, z: 8, core: 2. Of those that a mesh axis runs over, the one named last changes fastest.
Arguments:
- queries: bfloat16 [16384, 2048], P('sp', 'tp'), may hold values from -8 to 8
- keys: bfloat16 [16384, 512], P('sp'), may hold values from -6 to 6
- values: bfloat16 [16384, 512], P('sp'), may hold values from -6 to 6
- query_gain: float32 [2048], P('tp'), may hold values from 0.2 to 40
- key_gain: float32 [128], replicated, may hold values from 0.1 to 1.9
- out_weight: bfloat16 [2048, 2048], replicated, may hold values from -0.125 to 0.125
- residual: bfloat16 [16384, 2048], P(('sp', 'tp')), may hold values from -2 to 2
- norm_gain: float32 [2048], replicated, may hold values from 0.1 to 1.9
- route_experts: int32 [16384, 2], P(('sp', 'tp')), may hold values from 0 to 15, as said below
- expert_scores: float32 [16384, 2], P(('sp', 'tp')), may hold values from -9 to 9
- group_prob: float32 [16384], P(('sp', 'tp')), may hold values from 0.5 to 1
- w_gate: bfloat16 [16, 2048, 2048], P('sp', None, 'tp'), may hold values from -0.125 to 0.125
- w_up: bfloat16 [16, 2048, 2048], P('sp', None, 'tp'), may hold values from -0.125 to 0.125
- w_down: bfloat16 [16, 2048, 2048], P('sp', 'tp'), may hold values from -0.125 to 0.125
Outputs:
- mixed: bfloat16 [16384, 2048], P(('sp', 'tp'))
Inputs may be any that keep to these rules, and one draw needn't show every extreme that they name: `route_experts`: each row names 2 different experts of one group, expert e lying in group e // 8. In the rows of one device (aligned blocks of 64 rows) 5 * 8 rows choose one group and the others another; inside a group those rows are spread over its experts as evenly as whole numbers allow, so no expert is named by more than 10 rows of one device and some expert by exactly 10.
All inputs are finite; a program needn't handle non-finite values.
Results may differ from a plain program's by a relative error of at most 0.025.
Values may be sent and summed in bfloat16 or wider, within the bound.
No kernel may reach another device: no remote copies, remote signals or barrier semaphores. Data moves between devices by JAX's collectives and lax.ppermute only.
A program may use at most 128 MiB of HBM per device.

v0:
```python
import jax
import jax.numpy as jnp
from jax import lax
from jax.sharding import Mesh
from jax.sharding import PartitionSpec as P

GROUPS = 2
GRID_W = 64
TP = ("tp_0", "tp_1")
SP_TP = ("sp", "tp_0", "tp_1")


rope_base = 10000.0
norm_eps = 1e-06


def side_by_side(arrays, axis, dim, along):
    both = jnp.concatenate(arrays, axis=along)
    whole, at, gathered = (lax.all_gather(both, axis, axis=dim, tiled=True), 0, [])
    for a in arrays:
        gathered.append(lax.slice_in_dim(whole, at, at + a.shape[along], axis=along))
        at += a.shape[along]
    return tuple(gathered)


def cut_along(array, dim, devices):
    lengths = array.shape
    tiles = array.reshape(*lengths[:dim], devices, lengths[dim] // devices, *lengths[dim + 1 :])
    return jnp.moveaxis(tiles, dim, 0)


def laid_out(tiles, dim):
    tiles = jnp.moveaxis(tiles, 0, dim)
    lengths = tiles.shape
    return tiles.reshape(*lengths[:dim], lengths[dim] * lengths[dim + 1], *lengths[dim + 2 :])


def moved_by_axis(tiles, axes, turns):
    inside = tiles.shape[1:]
    whole = tiles.reshape(*(lax.axis_size(a) for a in axes), *inside)
    for k in turns:
        whole = lax.all_to_all(whole, axes[k], k, k, tiled=True)
    return whole.reshape(-1, *inside)


def one_axis_at_a_time(array, axes, turns, split_dim, concat_dim):
    tiles = cut_along(array, split_dim, lax.axis_size(axes))
    return laid_out(moved_by_axis(tiles, axes, turns), concat_dim)


def rope_tables(positions, head_size):
    quarter = head_size // 4
    frequency = rope_base ** (-jnp.arange(quarter, dtype=jnp.float32) * 4.0 / head_size)
    grid_row = (positions // GRID_W).astype(jnp.float32)
    grid_column = (positions % GRID_W).astype(jnp.float32)
    angles = jnp.concatenate(
        [grid_row[:, None] * frequency[None, :], grid_column[:, None] * frequency[None, :]], axis=1
    )
    return (jnp.cos(angles), jnp.sin(angles))


def rotate_pairs(vectors, cosine_table, sine_table):
    paired = vectors.reshape(vectors.shape[0], vectors.shape[1], vectors.shape[2] // 2, 2)
    leading = paired[..., 0]
    trailing = paired[..., 1]
    cosine_now = cosine_table[:, None, :]
    sine_now = sine_table[:, None, :]
    turned = jnp.stack(
        [leading * cosine_now - trailing * sine_now, leading * sine_now + trailing * cosine_now],
        axis=-1,
    )
    return turned.reshape(vectors.shape)


def head_norm(vectors, gain_row):
    factor = lax.rsqrt(jnp.mean(vectors * vectors, axis=-1, keepdims=True) + norm_eps)
    return vectors * factor * gain_row


def local(
    queries,
    keys,
    values,
    query_gain,
    key_gain,
    out_weight,
    residual,
    norm_gain,
    route_experts,
    expert_scores,
    group_prob,
    w_gate,
    w_up,
    w_down,
):
    span_tokens = queries.shape[0]
    head_size = key_gain.shape[0]
    local_heads = queries.shape[1] // head_size
    key_heads = keys.shape[1] // head_size
    model_size = lax.axis_size(TP)
    seq_size = lax.axis_size("sp")
    share = local_heads * model_size // key_heads
    model_index = lax.axis_index(TP)
    seq_index = lax.axis_index("sp")
    positions = seq_index * span_tokens + jnp.arange(span_tokens, dtype=jnp.int32)
    cosine_table, sine_table = rope_tables(positions, head_size)
    query_heads = queries.astype(jnp.float32).reshape(span_tokens, local_heads, head_size)
    query_heads = rotate_pairs(
        head_norm(query_heads, query_gain.reshape(1, local_heads, head_size)),
        cosine_table,
        sine_table,
    )
    query_rows = (
        query_heads.astype(jnp.bfloat16)
        .transpose(1, 0, 2)
        .reshape(local_heads * span_tokens, head_size)
    )
    shared_head = model_index * local_heads // share
    key_cols = lax.dynamic_slice_in_dim(keys, shared_head * head_size, head_size, 1)
    value_cols = lax.dynamic_slice_in_dim(values, shared_head * head_size, head_size, 1)
    key_rows = rotate_pairs(
        head_norm(
            key_cols.astype(jnp.float32).reshape(span_tokens, 1, head_size),
            key_gain.reshape(1, 1, head_size),
        ),
        cosine_table,
        sine_table,
    )
    key_rows = key_rows.reshape(span_tokens, head_size).astype(jnp.bfloat16)
    score_scale = head_size ** (-0.5)
    query_count = local_heads * span_tokens
    block_keys = span_tokens * max(1, 512 // span_tokens)

    def score_block(state, block_pair):
        running_max, row_total, weighted = state
        block_key_rows, block_value_rows = block_pair
        scores = (
            jnp.einsum("qd,kd->qk", query_rows, block_key_rows, preferred_element_type=jnp.float32)
            * score_scale
        )
        new_max = jnp.maximum(running_max, jnp.max(scores, axis=1))
        raised = jnp.exp(scores - new_max[:, None])
        fading = jnp.exp(running_max - new_max)
        row_total = row_total * fading + jnp.sum(raised, axis=1)
        weighted = weighted * fading[:, None] + jnp.dot(
            raised.astype(jnp.bfloat16), block_value_rows, preferred_element_type=jnp.float32
        )
        return ((new_max, row_total, weighted), None)

    initial = (
        jnp.full((query_count,), -jnp.inf, jnp.float32),
        jnp.zeros((query_count,), jnp.float32),
        jnp.zeros((query_count, head_size), jnp.float32),
    )
    piece_keys, piece_values = side_by_side((key_rows, value_cols), "sp", 0, 1)
    count = piece_keys.shape[0]
    stacked = (
        piece_keys.reshape(count // block_keys, block_keys, head_size),
        piece_values.reshape(count // block_keys, block_keys, head_size),
    )
    running_max, row_total, weighted = lax.scan(score_block, initial, stacked)[0]
    attended = (weighted / row_total[:, None]).astype(jnp.bfloat16)
    attended = (
        attended.reshape(local_heads, span_tokens, head_size)
        .transpose(1, 0, 2)
        .reshape(span_tokens, local_heads * head_size)
    )
    row_count = span_tokens // model_size
    all_heads = one_axis_at_a_time(attended, TP, (1, 0), 0, 1)
    update = jnp.dot(all_heads, out_weight, preferred_element_type=jnp.float32)
    updated = lax.optimization_barrier((residual.astype(jnp.float32) + update).astype(jnp.bfloat16))
    updated_wide = updated.astype(jnp.float32)
    normed = (
        updated_wide
        * lax.rsqrt(jnp.mean(updated_wide * updated_wide, axis=1, keepdims=True) + norm_eps)
        * norm_gain[None, :]
    ).astype(jnp.bfloat16)
    mixing = group_prob[:, None] * jax.nn.softmax(expert_scores, axis=1)
    local_experts = w_gate.shape[0]
    expert_total = local_experts * seq_size
    group_experts = expert_total // GROUPS
    top_count = route_experts.shape[1]
    capacity = (top_count * (5 * row_count // 8) + group_experts - 1) // group_experts
    model_width = updated_wide.shape[1]
    chosen_flat = route_experts.reshape(-1)
    expert_ids = jnp.arange(expert_total, dtype=jnp.int32)
    onehot = (chosen_flat[:, None] == expert_ids[None, :]).astype(jnp.int32)
    ordinal = jnp.sum((jnp.cumsum(onehot, axis=0) - onehot) * onehot, axis=1)
    slot_of = chosen_flat * capacity + ordinal
    slot_ids = jnp.arange(expert_total * capacity, dtype=jnp.int32)
    placing = jnp.any(
        slot_ids[:, None, None] == slot_of.reshape(row_count, top_count)[None, :, :], axis=2
    ).astype(jnp.bfloat16)
    outgoing = jnp.dot(placing, normed, preferred_element_type=jnp.float32).astype(jnp.bfloat16)
    outgoing = outgoing.reshape(seq_size, local_experts, capacity, model_width)
    arrived = lax.all_to_all(outgoing, "sp", split_axis=0, concat_axis=0, tiled=True)
    piece = lax.all_gather(arrived, TP, axis=0, tiled=True)
    gate_part = jnp.einsum("secd,edh->sech", piece, w_gate, preferred_element_type=jnp.float32)
    up_part = jnp.einsum("secd,edh->sech", piece, w_up, preferred_element_type=jnp.float32)
    hidden = (jax.nn.silu(gate_part) * up_part).astype(jnp.bfloat16)
    unit_rows = one_axis_at_a_time(hidden, TP, (1, 0), 0, 3)
    unit_block = w_down.shape[1]
    piece = lax.all_gather(w_down, TP, axis=1, tiled=True)
    piece_units = piece.shape[1]
    block_total = piece_units // unit_block
    columns = unit_rows
    columns = columns.reshape(
        columns.shape[0], columns.shape[1], columns.shape[2], block_total, unit_block
    )
    matrices = piece.reshape(piece.shape[0], block_total, unit_block, piece.shape[2])
    products = jnp.einsum(
        "secbh,ebhd->secbd", columns, matrices, preferred_element_type=jnp.float32
    )
    rounded = lax.optimization_barrier(products.astype(jnp.bfloat16)).astype(jnp.float32)
    returned = jnp.sum(rounded, axis=3).astype(jnp.bfloat16)
    result_rows = lax.all_to_all(returned, "sp", split_axis=0, concat_axis=0, tiled=True).reshape(
        expert_total * capacity, model_width
    )
    picked = result_rows[slot_of].astype(jnp.float32).reshape(row_count, top_count, model_width)
    combined = jnp.sum(picked * mixing[:, :, None], axis=1)
    return (updated_wide + combined).astype(jnp.bfloat16)


def solution(mesh):
    torus = Mesh(mesh.devices.reshape(mesh.shape["sp"], 8, 2), ("sp", "tp_0", "tp_1"))
    placed = (
        P("sp", TP),
        P("sp", None),
        P("sp", None),
        P(TP),
        P(),
        P(),
        P(SP_TP, None),
        P(),
        P(SP_TP, None),
        P(SP_TP, None),
        P(SP_TP),
        P("sp", None, TP),
        P("sp", None, TP),
        P("sp", TP, None),
    )
    return jax.shard_map(
        local, mesh=torus, in_specs=placed, out_specs=P(SP_TP, None), check_vma=False
    )
```

profile of v0, /device:TPU:1, one launch (start us, length us, event | category | flops | bytes accessed | tf_op | source)
XLA Modules:
  0.0 493.5 jit_solution(14839167092479442833)
XLA Ops:
  16.9 78.7 %all-gather.4.cloned.1.call-done = bf16[16384,256]{0,1:T(8,128)(2,1)} async-done(((bf16[1024,256]{0,1:T(8,128)(2,1)}), bf16[16384,256]{0,1:T(8,128)(2,1)}) %all-gather.4.cloned.1.call-update) | async-done | bytes 8388624 | tf_op jit(solution)/shard_map/all_gather | solution.py:19
  95.6 5.8 %fusion.64 = (bf16[16384,128]{0,1:T(8,128)(2,1)}, bf16[16384,128]{0,1:T(8,128)(2,1)}) fusion(bf16[16384,256]{0,1:T(8,128)(2,1)} %all-gather.4.cloned.1.call-done), kind=kLoop, calls=%fused_computation.102 | loop fusion | bytes 16777216 | tf_op jit(solution)/shard_map/slice | solution.py:21
  101.4 6.4 %copy.115 = bf16[16384,128]{1,0:T(8,128)(2,1)} copy(bf16[16384,128]{0,1:T(8,128)(2,1)} %get-tuple-element.123) | data formatting | bytes 8388608
  107.8 6.4 %copy.116 = bf16[16384,128]{1,0:T(8,128)(2,1)} copy(bf16[16384,128]{0,1:T(8,128)(2,1)} %get-tuple-element.122) | data formatting | bytes 8388608
  114.2 145.0 %while.15 = (s32[]{:T(128)}, f32[1024]{0:T(1024)S(1)}, f32[1024]{0:T(1024)S(1)}, f32[1024,128]{1,0:T(8,128)S(1)}, bf16[16,1024,128]{2,1,0:T(8,128)(2,1)}, /*inde...) while((s32[]{:T(128)}, f32[1024]{0:T(1024)S(1)}, ...), condition=%wide.region_5.6_spmd.clone, body=%wide.region_2.5_spmd.clone.sunk | while | flops 545657856 | bytes 31261828 | solution.py:161
  114.2 3.7 multiply_reduce_fusion.3
  117.8 3.1 fusion.81
  121.3 1.9 fusion.83
  123.3 3.6 multiply_reduce_fusion.3
  126.9 3.1 fusion.81
  132.3 3.6 multiply_reduce_fusion.3
  136.0 3.1 fusion.81
  139.4 1.9 fusion.83
  141.4 3.6 multiply_reduce_fusion.3
  145.0 3.1 fusion.81
  148.5 1.9 fusion.83
  150.4 3.6 multiply_reduce_fusion.3
  154.1 3.1 fusion.81
  159.5 3.6 multiply_reduce_fusion.3
  163.1 3.1 fusion.81
  166.6 1.9 fusion.83
  168.6 3.6 multiply_reduce_fusion.3
  172.2 3.1 fusion.81
  175.6 1.9 fusion.83
  177.6 3.6 multiply_reduce_fusion.3
  181.3 3.1 fusion.81
  186.7 3.6 multiply_reduce_fusion.3
  190.3 3.1 fusion.81
  193.8 1.9 fusion.83
  195.7 3.6 multiply_reduce_fusion.3
  199.4 3.1 fusion.81
  202.8 1.9 fusion.83
  204.8 3.6 multiply_reduce_fusion.3
  208.4 3.1 fusion.81
  213.8 3.6 multiply_reduce_fusion.3
  217.5 3.1 fusion.81
  220.9 1.9 fusion.83
  222.9 3.6 multiply_reduce_fusion.3
  226.5 3.1 fusion.81
  230.0 1.9 fusion.83
  232.0 3.6 multiply_reduce_fusion.3
  235.6 3.1 fusion.81
  241.0 3.6 multiply_reduce_fusion.3
  244.7 3.1 fusion.81
  250.1 3.6 multiply_reduce_fusion.3
  253.7 3.1 fusion.81
  257.2 1.9 fusion.83
  259.4 4.4 all_to_all.30
  264.5 6.7 %all-to-all-start.1 = ((bf16[8,2,64,128]{3,2,1,0:T(8,128)(2,1)}), bf16[8,2,64,128]{3,2,1,0:T(8,128)(2,1)S(1)}, u32[]{:S(2)}, u32[]{:S(2)}) async-start(bf16[8,2,64,128]{3,2,1,0:T(8,128)(2,1)} %copy.102), calls=%async_computation.1 | async-start | bytes 524288 | tf_op jit(solution)/shard_map/all_to_all | solution.py:42
  272.1 10.3 %all-to-all-done.1 = bf16[8,2,64,128]{3,2,1,0:T(8,128)(2,1)S(1)} async-done(((bf16[8,2,64,128]{3,2,1,0:T(8,128)(2,1)}), bf16[8,2,64,128]{3,2,1,0:T(8,128)(2,1)S(1)}, u32[]{:S(2)}, u32[]{:S(2)}) %all-to-all-start.1) | async-done | bytes 262176 | tf_op jit(solution)/shard_map/all_to_all | solution.py:42
  282.4 5.0 %fusion.22 = bf16[64,2048]{1,0:T(8,128)(2,1)S(1)} fusion(bf16[2048,2048]{1,0:T(8,128)(2,1)} %param.21, bf16[64,2048]{1,0:T(8,128)(2,1)S(1)} %copy-done.3, bf16[16,8,8,128]{3,2,1,0:T(8,128)(2,1)S(1)} %bitcast.109), kind=kOutput, calls=%fused_computation.29 | convolution fusion | flops 537264128 | bytes 9175040 | tf_op jit(solution)/shard_map/dot_general | solution.py:170
  288.2 20.2 %all_to_all.31 = bf16[16,1,10,2048]{3,2,1,0:T(8,128)(2,1)S(1)} all-to-all(bf16[16,1,10,2048]{3,2,1,0:T(8,128)(2,1)S(1)} %bitcast.107), channel_id=1, replica_groups=mesh['sp'=16,'tp_0'=8,'tp_1'=2] {'sp'}, dimensions={0} | all-to-all | bytes 1310720 | tf_op jit(solution)/shard_map/all_to_all | solution.py:196
  310.3 60.4 %all-gather.6.cloned.1.call-done = bf16[256,1,10,2048]{3,0,2,1:T(8,128)(2,1)} async-done(((bf16[16,1,10,2048]{3,0,2,1:T(8,128)(2,1)}), bf16[256,1,10,2048]{3,0,2,1:T(8,128)(2,1)}) %all-gather.6.cloned.1.call-update) | async-done | bytes 10485776 | tf_op jit(solution)/shard_map/all_gather | solution.py:197
  370.7 5.7 %fusion.23 = f32[256,1,10,128]{3,0,2,1:T(8,128)S(1)} fusion(bf16[256,1,10,2048]{3,0,2,1:T(8,128)(2,1)} %all-gather.6.cloned.1.call-done, bf16[1,2048,128]{2,1,0:T(8,128)(2,1)S(1)} %copy-done.9), kind=kOutput, calls=%fused_computation.30 | convolution fusion | flops 1342177280 | bytes 12320768 | tf_op jit(solution)/shard_map/secd,edh->sech/dot_general | solution.py:198
  377.8 2.9 fusion.32
  380.8 4.2 all_to_all.32
  386.0 4.5 all-to-all-start.4
  390.4 27.6 %all-to-all-done.4 = bf16[8,2,16,1,10,128]{5,2,1,4,3,0:T(8,128)(2,1)S(1)} async-done(((bf16[8,2,16,1,10,128]{5,2,1,4,3,0:T(8,128)(2,1)}), bf16[8,2,16,1,10,128]{5,2,1,4,3,0:T(8,128)(2,1)S(1)}, u32[]{:S(2)}, u32[]{:S(2)}) %all-to-all-start.4) | async-done | bytes 655392 | tf_op jit(solution)/shard_map/all_to_all | solution.py:42
  418.1 22.9 %all-gather.8.cloned.1.call-done = bf16[1,2048,2048]{2,1,0:T(8,128)(2,1)} async-done(((bf16[1,128,2048]{2,1,0:T(8,128)(2,1)}), bf16[1,2048,2048]{2,1,0:T(8,128)(2,1)}) %all-gather.8.cloned.1.call-update) | async-done | bytes 8388624 | tf_op jit(solution)/shard_map/all_gather | solution.py:203
  441.0 10.2 %convert_bitcast_fusion = bf16[16,1,10,16,2048]{4,0,2,3,1:T(8,128)(2,1)} fusion(bf16[16,10,16,128]{3,0,1,2:T(8,128)(2,1)S(1)} %bitcast.106, bf16[16,128,2048,1]{2,1,3,0:T(8,128)(2,1)} %bitcast.103), kind=kOutput, calls=%fused_computation.26 | convolution fusion | flops 1347420160 | bytes 19529728 | tf_op jit(solution)/shard_map/secbh,ebhd->secbd/dot_general | solution.py:211
  451.3 6.4 %reduce_sum.86 = bf16[16,10,2048]{2,0,1:T(8,128)(2,1)S(1)} reduce(bf16[16,1,10,16,2048]{4,0,2,3,1:T(8,128)(2,1)} %convert_bitcast_fusion, bf16[]{:T(256)} %constant.115.clone.1), dimensions={1,3}, to_apply=%region_10.11 | reduce | flops 4915200 | bytes 11141122 | tf_op jit(solution)/shard_map/reduce_sum | solution.py:215
  459.1 6.5 %all-to-all-start.5 = ((bf16[16,1,10,2048]{3,2,1,0:T(8,128)(2,1)}), bf16[16,1,10,2048]{3,2,1,0:T(8,128)(2,1)S(1)}, u32[]{:S(2)}, u32[]{:S(2)}) async-start(bf16[16,1,10,2048]{3,2,1,0:T(8,128)(2,1)} %copy.112), calls=%async_computation.5 | async-start | bytes 2097152 | tf_op jit(solution)/shard_map/all_to_all | solution.py:216
  466.5 15.5 %all-to-all-done.5 = bf16[16,1,10,2048]{3,2,1,0:T(8,128)(2,1)S(1)} async-done(((bf16[16,1,10,2048]{3,2,1,0:T(8,128)(2,1)}), bf16[16,1,10,2048]{3,2,1,0:T(8,128)(2,1)S(1)}, u32[]{:S(2)}, u32[]{:S(2)}) %all-to-all-start.5) | async-done | bytes 655392 | tf_op jit(solution)/shard_map/all_to_all | solution.py:216
  483.9 2.3 multiply_reduce_fusion.1
  (172 shorter events, 39.7 us)
Async XLA Ops:
  6.5 8.3 %copy-start = (bf16[1024,512]{1,0:T(8,128)(2,1)S(1)}, bf16[1024,512]{1,0:T(8,128)(2,1)}, u32[]{:S(2)}) copy-start(bf16[1024,512]{1,0:T(8,128)(2,1)} %param.18) | copy-start | bytes 3145732
  6.5 89.1 %all-gather.4.cloned.1.call-start = ((), (), s32[]{:S(2)}) async-start(), calls=%async_computation.6 | async-start | bytes 8912896 | tf_op jit(solution)/shard_map/all_gather | solution.py:19
  13.2 3.4 copy-start.6
  114.2 168.2 %copy-start.3 = (bf16[64,2048]{1,0:T(8,128)(2,1)S(1)}, bf16[64,2048]{1,0:T(8,128)(2,1)}, u32[]{:S(2)}) copy-start(bf16[64,2048]{1,0:T(8,128)(2,1)} %param.22) | copy-start | bytes 786436
  117.8 3.4 copy-start.2
  126.9 3.4 copy-start.2
  136.0 3.4 copy-start.2
  145.0 3.4 copy-start.2
  154.1 3.4 copy-start.2
  163.1 3.4 copy-start.2
  172.2 3.4 copy-start.2
  181.2 3.4 copy-start.2
  190.3 3.4 copy-start.2
  199.4 3.4 copy-start.2
  208.4 3.4 copy-start.2
  217.5 3.4 copy-start.2
  226.5 3.4 copy-start.2
  235.6 3.4 copy-start.2
  244.7 3.4 copy-start.2
  253.7 3.4 copy-start.2
  264.5 17.9 %all-to-all-start.1 = ((bf16[8,2,64,128]{3,2,1,0:T(8,128)(2,1)}), bf16[8,2,64,128]{3,2,1,0:T(8,128)(2,1)S(1)}, u32[]{:S(2)}, u32[]{:S(2)}) async-start(bf16[8,2,64,128]{3,2,1,0:T(8,128)(2,1)} %copy.102), calls=%async_computation.1 | async-start | bytes 524288 | tf_op jit(solution)/shard_map/all_to_all | solution.py:42
  271.2 99.5 %all-gather.6.cloned.1.call-start = ((), (), s32[]{:S(2)}) async-start(), calls=%async_computation.7 | async-start | bytes 11141120 | tf_op jit(solution)/shard_map/all_gather | solution.py:197
  282.4 5.2 %copy-start.5 = (f32[2048]{0:T(1024)S(1)}, f32[2048]{0:T(1024)}, u32[]{:S(2)}) copy-start(f32[2048]{0:T(1024)} %param.23) | copy-start | bytes 24580
  287.4 83.4 %copy-start.9 = (bf16[1,2048,128]{2,1,0:T(8,128)(2,1)S(1)}, bf16[1,2048,128]{2,1,0:T(8,128)(2,1)}, u32[]{:S(2)}) copy-start(bf16[1,2048,128]{2,1,0:T(8,128)(2,1)} %param.27) | copy-start | bytes 1572868
  309.6 131.5 %all-gather.8.cloned.1.call-start = ((), (), s32[]{:S(2)}) async-start(), calls=%async_computation.8 | async-start | bytes 8912896 | tf_op jit(solution)/shard_map/all_gather | solution.py:203
  310.3 66.2 %copy-start.10 = (bf16[1,2048,128]{2,1,0:T(8,128)(2,1)S(1)}, bf16[1,2048,128]{2,1,0:T(8,128)(2,1)}, u32[]{:S(2)}) copy-start(bf16[1,2048,128]{2,1,0:T(8,128)(2,1)} %param.28) | copy-start | bytes 1572868
  370.7 7.0 %copy-start.8 = (bf16[256,1,10,2048]{3,0,2,1:T(8,128)(2,1)S(1)}, bf16[256,1,10,2048]{3,0,2,1:T(8,128)(2,1)}, u32[]{:S(2)}) copy-start(bf16[256,1,10,2048]{3,0,2,1:T(8,128)(2,1)} %all-gather.6.cloned.1.call-done) | copy-start | bytes 31457284
  380.7 9.8 %copy-start.4 = (f32[64,2]{0,1:T(2,128)S(1)}, f32[64,2]{0,1:T(2,128)}, u32[]{:S(2)}) copy-start(f32[64,2]{0,1:T(2,128)} %param.25) | copy-start | bytes 1540
  386.0 32.0 %all-to-all-start.4 = ((bf16[8,2,16,1,10,128]{5,2,1,4,3,0:T(8,128)(2,1)}), bf16[8,2,16,1,10,128]{5,2,1,4,3,0:T(8,128)(2,1)S(1)}, u32[]{:S(2)}, u32[]{:S(2)}) async-start(bf16[8,2,16,1,10,128]{5,2,1,4,3,0:T(8,128)(2,1)} %copy.110), calls=%async_computation.4 | async-start | bytes 1310720 | tf_op jit(solution)/shard_map/all_to_all | solution.py:42
  451.3 14.5 %copy-start.7 = (f32[64]{0:T(128)S(1)}, f32[64]{0:T(128)}, u32[]{:S(2)}) copy-start(f32[64]{0:T(128)} %param.26) | copy-start | bytes 772
  459.1 23.0 %all-to-all-start.5 = ((bf16[16,1,10,2048]{3,2,1,0:T(8,128)(2,1)}), bf16[16,1,10,2048]{3,2,1,0:T(8,128)(2,1)S(1)}, u32[]{:S(2)}, u32[]{:S(2)}) async-start(bf16[16,1,10,2048]{3,2,1,0:T(8,128)(2,1)} %copy.112), calls=%async_computation.5 | async-start | bytes 2097152 | tf_op jit(solution)/shard_map/all_to_all | solution.py:216
  482.1 4.9 copy-start.1
Sparse Core Ops, SparseCore 0:
  16.1 79.4 all-gather.3
  309.7 60.9 all-gather.5
  372.6 68.4 all-gather.7
where the time goes:
time: 495 us; the launch traced here: 494 us
  waiting for transfers between devices  216 us (44%)
  matrix products  114 us (23%)
  other arithmetic  66.7 us (13%)
  local copies, waits for them, and re-layouts  36.5 us (7%)
  blocking collectives  28.7 us (6%)
  starting transfers between devices  18 us (4%)
  between operations  13.6 us (3%)
    all_gather x1, waiting for transfers between devices, side_by_side(): lax.all_gather(both, axis, axis=dim, tiled=True)  78.7 us
    all_gather x1, waiting for transfers between devices, local(): piece = lax.all_gather(arrived, TP, axis=0, tiled=True)  60.4 us
    dot_general x16, matrix products, score_block(): jnp.einsum('qd,kd->qk', query_rows, block_key_rows, preferred_element_typ...  58.2 us
    reduce_sum x16, other arithmetic, score_block(): row_total = row_total * fading + jnp.sum(raised, axis=1)  49.1 us
    all_to_all x2, waiting for transfers between devices, moved_by_axis(): whole = lax.all_to_all(whole, axes[k], k, k, tiled=True)  37.9 us
    dot_general x16, matrix products, score_block(): jnp.dot(raised.astype(jnp.bfloat16), block_value_rows, preferred_element_...  31.1 us
    all_gather x1, waiting for transfers between devices, local(): piece = lax.all_gather(w_down, TP, axis=1, tiled=True)  22.9 us
    all_to_all x1, blocking collectives, local(): lax.all_to_all(outgoing, 'sp', split_axis=0, concat_axis=0, tiled=True)  20.2 us
  transfers between devices with their start and end apart: 6, of which 6 were waited for; matrix products, arithmetic and copies ran while one was open for 2% of the time, Pallas kernels for 0%

commit v1 on v0

v1 whole, which is shorter than its diff:
```python
import functools
import math

import jax
import jax.numpy as jnp
from jax import lax
from jax.experimental import pallas as pl
from jax.experimental.pallas import tpu as pltpu
from jax.sharding import Mesh
from jax.sharding import PartitionSpec as P

GRID_W = 64
HEAD = 128
SP = "sp"
TP = ("z", "core")
SP_TP = ("sp", "z", "core")
rope_base = 10000.0
norm_eps = 1e-06
f32 = jnp.float32
bf16 = jnp.bfloat16


def dot(a, b):
    return jnp.dot(a, b, preferred_element_type=f32)


def prep_kernel(where_ref, q_ref, k_ref, v_ref, qg_ref, kg_ref, cos_ref, sin_ref, q_out, kv_out):
    lane = lax.broadcasted_iota(jnp.int32, (GRID_W, HEAD), 1)
    even = lane % 2 == 0
    from_row = lane < HEAD // 2
    col_cos = cos_ref[16:, :]
    col_sin = sin_ref[16:, :]

    def turn(vectors, gain, row_cos, row_sin):
        mean = jnp.mean(vectors * vectors, axis=-1, keepdims=True)
        u = vectors * lax.rsqrt(mean + norm_eps) * gain
        swapped = jnp.where(even, pltpu.roll(u, HEAD - 1, 1), pltpu.roll(u, 1, 1))
        cosine = jnp.where(from_row, row_cos, col_cos)
        sine = jnp.where(from_row, row_sin, col_sin)
        return u * cosine + swapped * sine

    for r in range(q_ref.shape[0] // GRID_W):
        rows = slice(r * GRID_W, (r + 1) * GRID_W)
        q_out[rows, :] = turn(
            q_ref[rows, :].astype(f32), qg_ref[...], cos_ref[r : r + 1, :], sin_ref[r : r + 1, :]
        ).astype(bf16)
    half = k_ref.shape[0] // GRID_W
    first = where_ref[0] * half
    for r in range(half):
        rows = slice(r * GRID_W, (r + 1) * GRID_W)
        row_cos = cos_ref[pl.ds(first + r, 1), :]
        row_sin = sin_ref[pl.ds(first + r, 1), :]
        kv_out[rows, :HEAD] = turn(
            k_ref[rows, :].astype(f32), kg_ref[...], row_cos, row_sin
        ).astype(bf16)
    kv_out[:, HEAD:] = v_ref[...]


def prep(where, queries, keys, values, query_gain, key_gain, cosine, sine):
    tokens = queries.shape[0]
    half = tokens // 2
    whole = lambda shape: pl.BlockSpec(shape, lambda i, w: (0, 0))
    part = pl.BlockSpec((half, HEAD), lambda i, w: (w[0], w[1]))
    return pl.pallas_call(
        prep_kernel,
        grid_spec=pltpu.PrefetchScalarGridSpec(
            num_scalar_prefetch=1,
            grid=(1,),
            in_specs=[
                whole((tokens, HEAD)),
                part,
                part,
                whole((1, HEAD)),
                whole((1, HEAD)),
                whole(cosine.shape),
                whole(sine.shape),
            ],
            out_specs=[whole((tokens, HEAD)), whole((half, 2 * HEAD))],
        ),
        out_shape=[
            jax.ShapeDtypeStruct((tokens, HEAD), bf16),
            jax.ShapeDtypeStruct((half, 2 * HEAD), bf16),
        ],
        name="prep",
    )(where, queries, keys, values, query_gain, key_gain, cosine, sine)


BQ = 256
CK = 1024


def attend_kernel(where_ref, own_ref, sib_ref, kv_ref, keep_ref, send_ref, kk, vv):
    blocks, rows, _ = kv_ref.shape

    @pl.when((pl.program_id(0) == 0) & (pl.program_id(1) == 0))
    def _():
        def fill(b, carry):
            span = pl.ds(pl.multiple_of(b * rows, rows), rows)
            k = kv_ref[b, :, :HEAD]
            kk[span, :HEAD] = k
            kk[span, HEAD:] = k
            vv[span, :HEAD] = kv_ref[b, :, HEAD:]
            vv[span, HEAD:] = jnp.ones((rows, HEAD), bf16)
            return carry

        lax.fori_loop(0, blocks, fill, 0)

    q = jnp.where(pl.program_id(0) == 0, own_ref[...].astype(f32), sib_ref[...].astype(f32))
    scaled = q * (HEAD ** (-0.5) * math.log2(math.e))
    high = scaled.astype(bf16)
    low = (scaled - high.astype(f32)).astype(bf16)
    pair = jnp.concatenate([high, low], axis=1)
    top = acc = None
    for j in range(blocks * rows // CK):
        span = slice(j * CK, (j + 1) * CK)
        s = lax.dot_general(
            pair, kk[span, :], (((1,), (1,)), ((), ())), preferred_element_type=f32
        )
        block_top = jnp.max(s, axis=1, keepdims=True)
        new_top = block_top if top is None else jnp.maximum(top, block_top)
        raised = jnp.exp2(s - new_top).astype(bf16)
        part = dot(raised, vv[span, :])
        acc = part if top is None else acc * jnp.exp2(top - new_top) + part
        top = new_top
    total = acc[:, HEAD:]
    normal = acc[:, :HEAD] / total
    level = top + jnp.log2(total)
    first_core = where_ref[0] == 0
    for z in range(BQ // 128):
        a = slice(z * 128, z * 128 + 64)
        b = slice(z * 128 + 64, z * 128 + 128)
        keep_ref[0, z, :, :HEAD] = jnp.where(first_core, normal[a], normal[b])
        keep_ref[0, z, :, HEAD:] = jnp.where(first_core, level[a], level[b])
        send_ref[0, z, :, :HEAD] = jnp.where(first_core, normal[b], normal[a])
        send_ref[0, z, :, HEAD:] = jnp.where(first_core, level[b], level[a])


def attend(where, own, sib, kv):
    tokens = own.shape[0]
    blocks, rows, _ = kv.shape
    q_spec = pl.BlockSpec((BQ, HEAD), lambda h, i, w: (i, 0))
    out_spec = pl.BlockSpec((1, BQ // 128, 64, 2 * HEAD), lambda h, i, w: (h, i, 0, 0))
    out = jax.ShapeDtypeStruct((2, tokens // 128, 64, 2 * HEAD), f32)
    return pl.pallas_call(
        attend_kernel,
        grid_spec=pltpu.PrefetchScalarGridSpec(
            num_scalar_prefetch=1,
            grid=(2, tokens // BQ),
            in_specs=[
                q_spec,
                q_spec,
                pl.BlockSpec((blocks, rows, 2 * HEAD), lambda h, i, w: (0, 0, 0)),
            ],
            out_specs=[out_spec, out_spec],
            scratch_shapes=[
                pltpu.VMEM((blocks * rows, 2 * HEAD), bf16),
                pltpu.VMEM((blocks * rows, 2 * HEAD), bf16),
            ],
        ),
        out_shape=[out, out],
        compiler_params=pltpu.CompilerParams(vmem_limit_bytes=48 * 1024 * 1024),
        name="attend",
    )(where, own, sib, kv)


def merge_kernel(where_ref, keep_ref, got_ref, out_ref):
    def merged(mine, other):
        level = jnp.maximum(mine[:, HEAD:], other[:, HEAD:])
        a = jnp.exp2(mine[:, HEAD:] - level)
        b = jnp.exp2(other[:, HEAD:] - level)
        return (mine[:, :HEAD] * a + other[:, :HEAD] * b) / (a + b)

    first_core = where_ref[0] == 0
    for z in range(keep_ref.shape[1]):
        own = merged(keep_ref[0, z], got_ref[1, z])
        sib = merged(keep_ref[1, z], got_ref[0, z])
        out_ref[z, :, :HEAD] = jnp.where(first_core, own, sib).astype(bf16)
        out_ref[z, :, HEAD:] = jnp.where(first_core, sib, own).astype(bf16)


def merge(where, keep, got):
    _, z, rows, _ = keep.shape
    return pl.pallas_call(
        merge_kernel,
        grid_spec=pltpu.PrefetchScalarGridSpec(
            num_scalar_prefetch=1,
            grid=(1,),
            in_specs=[pl.BlockSpec(keep.shape, lambda i, w: (0, 0, 0, 0))] * 2,
            out_specs=pl.BlockSpec((z, rows, 2 * HEAD), lambda i, w: (0, 0, 0)),
        ),
        out_shape=jax.ShapeDtypeStruct((z, rows, 2 * HEAD), bf16),
        name="merge",
    )(where, keep, got)


def swap_matrix(experts, blocks):
    count = experts * blocks * 2
    row = lax.broadcasted_iota(jnp.int32, (count, count), 0)
    col = lax.broadcasted_iota(jnp.int32, (count, count), 1)
    a, b, j = row // (blocks * 2), (row // 2) % blocks, row % 2
    return jnp.where(col == b * (experts * 2) + a * 2 + j, 1.0, 0.0).astype(bf16)


def pack(rows_of, out_ref):
    peers = out_ref.shape[0]
    blocks = 16
    tails = []
    for k in range(blocks):
        block = rows_of(k)
        head = block[: peers * 8].reshape(peers, 8, HEAD)
        out_ref[:, k * 8 : (k + 1) * 8, :] = head.astype(bf16)
        tails.append(block[peers * 8 :])
    tail = jnp.concatenate(tails, axis=0).astype(bf16)
    turned = dot(swap_matrix(peers, blocks), tail)
    out_ref[:, blocks * 8 :, :] = turned.reshape(peers, blocks * 2, HEAD).astype(bf16)


def unpack(in_ref, store):
    peers = in_ref.shape[0]
    blocks = 16
    tail = in_ref[:, blocks * 8 :, :].astype(f32).reshape(peers * blocks * 2, HEAD).astype(bf16)
    turned = dot(swap_matrix(blocks, peers), tail)
    for k in range(blocks):
        head = in_ref[:, k * 8 : (k + 1) * 8, :].astype(f32).reshape(peers * 8, HEAD)
        store(k, jnp.concatenate([head, turned[k * peers * 2 : (k + 1) * peers * 2]], axis=0))


def slot_of(expert, ordinal, experts):
    return jnp.where(ordinal < 8, expert * 8 + ordinal, experts * 8 + expert * 2 + ordinal - 8)


def project_kernel(a_ref, w_ref, res_ref, gain_ref, route_ref, route_t_ref, upd_ref, out_ref, acc):
    step = pl.program_id(0)
    part = dot(a_ref[0], w_ref[...])

    @pl.when(step == 0)
    def _():
        acc[...] = part

    @pl.when(step > 0)
    def _():
        acc[...] += part

    @pl.when(step == pl.num_programs(0) - 1)
    def _():
        updated = (res_ref[...].astype(f32) + acc[...]).astype(bf16)
        upd_ref[...] = updated
        wide = updated.astype(f32)
        mean = jnp.mean(wide * wide, axis=1, keepdims=True)
        normed = (wide * lax.rsqrt(mean + norm_eps) * gain_ref[...]).astype(bf16)
        rows = wide.shape[0]
        experts = out_ref.shape[0]
        earlier = lax.broadcasted_iota(jnp.int32, (rows, rows), 0)
        later = lax.broadcasted_iota(jnp.int32, (rows, rows), 1)
        slots = lax.broadcasted_iota(jnp.int32, (experts * 10, rows), 0)
        placing = jnp.zeros((experts * 10, rows), f32)
        for t in range(2):
            mine = route_t_ref[t : t + 1, :]
            ordinal = jnp.zeros((1, rows), jnp.int32)
            for u in range(2):
                before = (earlier < later) if u >= t else (earlier <= later)
                same = route_ref[:, u : u + 1] == mine
                ordinal += jnp.sum(jnp.where(before & same, 1, 0), axis=0, keepdims=True)
            placing += jnp.where(slots == slot_of(mine, ordinal, experts), 1.0, 0.0)
        sent = dot(placing.astype(bf16), normed)
        pack(lambda k: sent[:, k * HEAD : (k + 1) * HEAD], out_ref)


def project(attended, out_weight, residual, norm_gain, route, route_t, peers):
    steps, rows, depth = attended.shape
    width = out_weight.shape[1]
    whole = lambda a: pl.BlockSpec(a.shape, lambda i: (0,) * a.ndim)
    return pl.pallas_call(
        project_kernel,
        grid=(steps,),
        in_specs=[
            pl.BlockSpec((1, rows, depth), lambda i: (i, 0, 0)),
            pl.BlockSpec((depth, width), lambda i: (i, 0)),
            whole(residual),
            whole(norm_gain),
            whole(route),
            whole(route_t),
        ],
        out_specs=[
            pl.BlockSpec((rows, width), lambda i: (0, 0)),
            pl.BlockSpec((peers, 160, HEAD), lambda i: (0, 0, 0)),
        ],
        out_shape=[
            jax.ShapeDtypeStruct((rows, width), bf16),
            jax.ShapeDtypeStruct((peers, 160, HEAD), bf16),
        ],
        scratch_shapes=[pltpu.VMEM((rows, width), f32)],
        name="project",
    )(attended, out_weight, residual, norm_gain, route, route_t)


def hidden_kernel(in_ref, gate_ref, up_ref, hid_ref, x):
    @pl.when(pl.program_id(0) == 0)
    def _():
        def store(k, block):
            x[:, k * HEAD : (k + 1) * HEAD] = block.astype(bf16)

        unpack(in_ref, store)

    gate = dot(x[...], jnp.concatenate([gate_ref[0], gate_ref[1]], axis=1))
    up = dot(x[...], jnp.concatenate([up_ref[0], up_ref[1]], axis=1))
    hid_ref[...] = (gate / (1.0 + jnp.exp(-gate)) * up).astype(bf16)


def hidden(arrived, gate, up):
    blocks, width, units = gate.shape
    w_spec = pl.BlockSpec((2, width, units), lambda i: (i, 0, 0))
    return pl.pallas_call(
        hidden_kernel,
        grid=(blocks // 2,),
        in_specs=[pl.BlockSpec(arrived.shape, lambda i: (0, 0, 0)), w_spec, w_spec],
        out_specs=pl.BlockSpec((160, 2 * units), lambda i: (0, i)),
        out_shape=jax.ShapeDtypeStruct((160, blocks * units), bf16),
        scratch_shapes=[pltpu.VMEM((160, width), bf16)],
        name="hidden",
    )(arrived, gate, up)


def down_kernel(hid_ref, down_ref, out_ref, acc):
    step = pl.program_id(0)
    weights = jnp.concatenate([down_ref[0], down_ref[1]], axis=0)
    part = dot(hid_ref[...], weights)

    @pl.when(step == 0)
    def _():
        acc[...] = part

    @pl.when(step > 0)
    def _():
        acc[...] += part

    @pl.when(step == pl.num_programs(0) - 1)
    def _():
        pack(lambda k: acc[:, k * HEAD : (k + 1) * HEAD], out_ref)


def down(hid, weights, peers):
    blocks, units, width = weights.shape
    return pl.pallas_call(
        down_kernel,
        grid=(blocks // 2,),
        in_specs=[
            pl.BlockSpec((160, 2 * units), lambda i: (0, i)),
            pl.BlockSpec((2, units, width), lambda i: (i, 0, 0)),
        ],
        out_specs=pl.BlockSpec((peers, 160, HEAD), lambda i: (0, 0, 0)),
        out_shape=jax.ShapeDtypeStruct((peers, 160, HEAD), bf16),
        scratch_shapes=[pltpu.VMEM((160, width), f32)],
        name="down",
    )(hid, weights)


def mix_kernel(in_ref, upd_ref, route_ref, route_t_ref, score_ref, prob_ref, out_ref):
    rows = upd_ref.shape[0]
    experts = in_ref.shape[0]
    later = lax.broadcasted_iota(jnp.int32, (rows, rows), 0)
    earlier = lax.broadcasted_iota(jnp.int32, (rows, rows), 1)
    slots = lax.broadcasted_iota(jnp.int32, (rows, experts * 10), 1)
    picks = []
    for t in range(2):
        mine = route_ref[:, t : t + 1]
        ordinal = jnp.zeros((rows, 1), jnp.int32)
        for u in range(2):
            before = (earlier < later) if u >= t else (earlier <= later)
            same = route_t_ref[u : u + 1, :] == mine
            ordinal += jnp.sum(jnp.where(before & same, 1, 0), axis=1, keepdims=True)
        picks.append(jnp.where(slots == slot_of(mine, ordinal, experts), 1.0, 0.0).astype(bf16))
    scores = score_ref[...]
    raised = jnp.exp(scores - jnp.max(scores, axis=1, keepdims=True))
    mixing = prob_ref[...] * (raised / jnp.sum(raised, axis=1, keepdims=True))

    def store(k, block):
        block = block.astype(bf16)
        cols = slice(k * HEAD, (k + 1) * HEAD)
        combined = sum(dot(picks[t], block) * mixing[:, t : t + 1] for t in range(2))
        out_ref[:, cols] = (upd_ref[:, cols].astype(f32) + combined).astype(bf16)

    unpack(in_ref, store)


def mix(returned, updated, route, route_t, scores, prob):
    return pl.pallas_call(
        mix_kernel,
        out_shape=jax.ShapeDtypeStruct(updated.shape, bf16),
        name="mix",
    )(returned, updated, route, route_t, scores, prob)


def local(
    queries,
    keys,
    values,
    query_gain,
    key_gain,
    out_weight,
    residual,
    norm_gain,
    route_experts,
    expert_scores,
    group_prob,
    w_gate,
    w_up,
    w_down,
):
    peers = lax.axis_size(SP)
    core = lax.axis_index("core")
    z = lax.axis_index("z")
    seq = lax.axis_index(SP)
    tokens = queries.shape[0]

    gate = lax.all_gather(w_gate[0], TP)
    up = lax.all_gather(w_up[0], TP)
    down_weight = lax.all_gather(w_down[0], TP)

    where = jnp.stack([core, z // 2]).astype(jnp.int32)
    lane = jnp.arange(HEAD, dtype=jnp.int32)
    pair = (lane // 2) % (HEAD // 4)
    frequency = rope_base ** (-pair.astype(f32) * 4.0 / HEAD)
    grid_rows = tokens // GRID_W
    place = jnp.arange(grid_rows + GRID_W, dtype=jnp.int32)
    place = jnp.where(place < grid_rows, seq * grid_rows + place, place - grid_rows)
    angles = place.astype(f32)[:, None] * frequency[None, :]
    cosine = jnp.cos(angles)
    sine = jnp.sin(angles) * jnp.where(lane % 2 == 0, -1.0, 1.0)[None, :]

    own, kv = prep(
        where, queries, keys, values, query_gain[None, :], key_gain[None, :], cosine, sine
    )
    sib = lax.ppermute(own, "core", ((0, 1), (1, 0)))
    kv_all = lax.all_to_all(
        jnp.broadcast_to(kv[None], (peers, *kv.shape)), SP, 0, 0, tiled=True
    )
    keep, send = attend(where, own, sib, kv_all)
    got = lax.ppermute(send, "core", ((0, 1), (1, 0)))
    attended = lax.all_to_all(merge(where, keep, got), "z", 0, 0, tiled=True)
    route_t = route_experts.T
    updated, outgoing = project(
        attended, out_weight, residual, norm_gain[None, :], route_experts, route_t, peers
    )
    arrived = lax.all_to_all(outgoing, SP, 0, 0, tiled=True)
    hid = hidden(arrived, gate, up)
    result = down(hid, down_weight, peers)
    returned = lax.all_to_all(result, SP, 0, 0, tiled=True)
    return mix(
        returned, updated, route_experts, route_t, expert_scores, group_prob[:, None]
    )


def solution(mesh):
    torus = Mesh(mesh.devices.reshape(mesh.shape["sp"], 8, 2), ("sp", "z", "core"))
    placed = (
        P(SP, TP),
        P(SP, None),
        P(SP, None),
        P(TP),
        P(),
        P(),
        P(SP_TP, None),
        P(),
        P(SP_TP, None),
        P(SP_TP, None),
        P(SP_TP),
        P(SP, None, TP),
        P(SP, None, TP),
        P(SP, TP, None),
    )
    return jax.shard_map(
        local, mesh=torus, in_specs=placed, out_specs=P(SP_TP, None), check_vma=False
    )
```

time: 495 us -> 222 us (0.45)
  waiting for transfers between devices: 216 us -> 91.2 us
  matrix products: 114 us -> 0 us
  Pallas kernels: 0 us -> 67.2 us
  other arithmetic: 66.7 us -> 1.46 us
  local copies, waits for them, and re-layouts: 36.5 us -> 9.11 us
  blocking collectives: 28.7 us -> 15.1 us
  starting transfers between devices: 18 us -> 23.3 us
    all_gather x3, waiting for transfers between devices: 162 us -> 2.49 us  [the longest x1 2.48 us: local(): down_weight = lax.all_gather(w_down[0], TP)]
    dot_general x37 -> x0, matrix products: 114 us -> none  [the longest x16 58.2 us: score_block(): jnp.einsum('qd,kd->qk', query_rows, block_key_rows, preferred_element_typ...]
    pallas_call x0 -> x7, Pallas kernels: none -> 67.2 us  [the longest x1 27.1 us: attend(): pl.pallas_call(attend_kernel, grid_spec=pltpu.PrefetchScalarGridSpec(num_...]
    reduce_sum x23 -> x0, other arithmetic: 60.6 us -> none  [the longest x16 49.1 us: score_block(): row_total = row_total * fading + jnp.sum(raised, axis=1)]
    all_to_all x3, waiting for transfers between devices: 53.4 us -> 83 us  [the longest x1 60.2 us: local(): lax.all_to_all(jnp.broadcast_to(kv[None], (peers, *kv.shape)), SP, 0, 0,...]
    all_to_all x3 -> x1, blocking collectives: 28.7 us -> 15.1 us  [local(): arrived = lax.all_to_all(outgoing, SP, 0, 0, tiled=True)]
    unnamed x25 -> x20, local copies, waits for them, and re-layouts: 14.5 us -> 5.01 us
    slice x2 -> x0, local copies, waits for them, and re-layouts: 6.62 us -> none  [the longest x1 5.81 us: side_by_side(): lax.slice_in_dim(whole, at, at + a.shape[along], axis=along)]
  transfers between devices with their start and end apart: 6 -> 8, of which waited for: 6 -> 6; matrix products, arithmetic and copies ran while one was open for 2% -> 3% of each run, Pallas kernels for 0% -> 25%
where the time goes in v1:
time: 222 us; the launch traced here: 221 us
  waiting for transfers between devices  91.2 us (41%)
  Pallas kernels  67.2 us (30%)
  starting transfers between devices  23.3 us (10%)
  blocking collectives  15.1 us (7%)
  between operations  13.2 us (6%)
  local copies, waits for them, and re-layouts  9.11 us (4%)
    all_to_all x1, waiting for transfers between devices, local(): lax.all_to_all(jnp.broadcast_to(kv[None], (peers, *kv.shape)), SP, 0, 0,...  60.2 us
    pallas_call x1, Pallas kernels, attend(): pl.pallas_call(attend_kernel, grid_spec=pltpu.PrefetchScalarGridSpec(num_...  27.1 us
    all_to_all x1, blocking collectives, local(): arrived = lax.all_to_all(outgoing, SP, 0, 0, tiled=True)  15.1 us
    all_to_all x1, waiting for transfers between devices, local(): attended = lax.all_to_all(merge(where, keep, got), 'z', 0, 0, tiled=True)  11.9 us
    pallas_call x1, Pallas kernels, hidden(): pl.pallas_call(hidden_kernel, grid=(blocks // 2,), in_specs=[pl.BlockSpec...  10.9 us
    all_to_all x1, waiting for transfers between devices, local(): returned = lax.all_to_all(result, SP, 0, 0, tiled=True)  10.8 us
    pallas_call x1, Pallas kernels, project(): pl.pallas_call(project_kernel, grid=(steps,), in_specs=[pl.BlockSpec((1,...  9.04 us
    pallas_call x1, Pallas kernels, down(): pl.pallas_call(down_kernel, grid=(blocks // 2,), in_specs=[pl.BlockSpec((...  8.91 us
  transfers between devices with their start and end apart: 8, of which 6 were waited for; matrix products, arithmetic and copies ran while one was open for 3% of the time, Pallas kernels for 25%

profile of v1, /device:TPU:1, one launch (start us, length us, event | category | flops | bytes accessed | tf_op | source)
XLA Modules:
  0.0 220.6 jit_solution(18068215949728466306)
XLA Ops:
  6.5 0.0 all-gather.4.cloned.1.call-start
  6.5 0.7 all-gather.4.cloned.1.call-update
  7.3 0.0 all-gather.6.cloned.1.call-start
  7.3 0.7 all-gather.6.cloned.1.call-update
  8.0 0.0 all-gather.8.cloned.1.call-start
  8.1 0.7 all-gather.8.cloned.1.call-update
  8.8 0.6 pad_add_fusion.where_ref
  9.3 0.0 copy-start.2
  9.4 0.9 fusion
  10.2 5.2 %prep.1 = (bf16[1024,128]{1,0:T(8,128)(2,1)}, bf16[512,256]{1,0:T(8,128)(2,1)}) custom-call(s32[2]{0:T(128)} %pad_add_fusion.where_ref, bf16[1024,128]{1,0:T(8,128)(2,1)} %q_ref.1, bf16[1024,512]{1,0:T(8,128)(2,1)} %k_ref.1, bf16[1024,512]{1,0:T(8,128)(2,1)} %v_ref.1, f32[1,128]{1,0:T(1,128)} %bitcast.10, f32[1,128]{1,0:T(1,128)} %bitcast.11, ...), custom_call_target="tpu_custom_call" | custom-call | tf_op jit(solution)/shard_map/prep/pallas_call | solution.py:64
  15.4 0.0 copy-start.1
  15.4 3.4 %broadcast_in_dim.33 = bf16[16,512,256]{2,1,0:T(8,128)(2,1)} broadcast(bf16[512,256]{1,0:T(8,128)(2,1)} %get-tuple-element.12), dimensions={1,2} | broadcast | bytes 4456448 | tf_op jit(solution)/shard_map/broadcast_in_dim | solution.py:436
  18.8 0.0 copy-start.6
  18.8 7.8 %all-to-all-start = ((bf16[16,512,256]{2,1,0:T(8,128)(2,1)}), bf16[16,512,256]{2,1,0:T(8,128)(2,1)}, u32[]{:S(2)}, u32[]{:S(2)}) async-start(bf16[16,512,256]{2,1,0:T(8,128)(2,1)} %broadcast_in_dim.33), calls=%async_computation | async-start | bytes 8388608 | tf_op jit(solution)/shard_map/all_to_all | solution.py:435
  26.6 0.0 copy-done.1
  26.6 1.0 collective-permute-start
  27.7 1.2 collective-permute-done.sib_ref
  28.8 60.2 %all-to-all-done.kv_ref = bf16[16,512,256]{2,1,0:T(8,128)(2,1)} async-done(((bf16[16,512,256]{2,1,0:T(8,128)(2,1)}), bf16[16,512,256]{2,1,0:T(8,128)(2,1)}, u32[]{:S(2)}, u32[]{:S(2)}) %all-to-all-start) | async-done | bytes 4194336 | tf_op jit(solution)/shard_map/all_to_all | solution.py:435
  89.1 0.0 copy-done.2
  89.1 27.1 %attend.1 = (f32[2,8,64,256]{3,2,1,0:T(8,128)S(1)}, f32[2,8,64,256]{3,2,1,0:T(8,128)S(1)}) custom-call(s32[2]{0:T(128)S(1)} %copy-done.2, bf16[1024,128]{1,0:T(8,128)(2,1)S(1)} %copy-done.1, bf16[1024,128]{1,0:T(8,128)(2,1)S(1)} %collective-permute-done.sib_ref, bf16[16,512,256]{2,1,0:T(8,128)(2,1)} %all-to-all-done.kv_ref), custom_call_target="tpu_custom_call" | custom-call | tf_op jit(solution)/shard_map/attend/pallas_call | solution.py:144
  116.2 0.0 copy-start
  116.2 1.0 copy-done
  117.3 1.8 collective-permute-start.1
  119.0 2.5 %collective-permute-done.1.got_ref = f32[2,8,64,256]{3,2,1,0:T(8,128)S(1)} collective-permute-done((f32[2,8,64,256]{3,2,1,0:T(8,128)S(1)}, f32[2,8,64,256]{3,2,1,0:T(8,128)S(1)}, u32[]{:S(2)}, u32[]{:S(2)}) %collective-permute-start.1) | collective-permute-done | bytes 1048608 | tf_op jit(solution)/shard_map/ppermute | solution.py:439
  121.5 0.0 copy-start.4
  121.5 1.0 copy-done.4
  122.5 3.2 %merge.1 = bf16[8,64,256]{2,1,0:T(8,128)(2,1)} custom-call(s32[2]{0:T(128)} %pad_add_fusion.where_ref, f32[2,8,64,256]{3,2,1,0:T(8,128)} %copy-done, f32[2,8,64,256]{3,2,1,0:T(8,128)} %copy-done.4), custom_call_target="tpu_custom_call" | custom-call | tf_op jit(solution)/shard_map/merge/pallas_call | solution.py:183
  125.7 8.2 %all-to-all-start.1 = ((bf16[8,64,256]{2,1,0:T(8,128)(2,1)}), bf16[8,64,256]{2,1,0:T(8,128)(2,1)S(1)}, u32[]{:S(2)}, u32[]{:S(2)}) async-start(bf16[8,64,256]{2,1,0:T(8,128)(2,1)} %merge.1), calls=%async_computation.1 | async-start | bytes 524288 | tf_op jit(solution)/shard_map/all_to_all | solution.py:440
  133.9 0.0 copy-done.6
  133.9 0.7 copy.19.route_ref
  134.6 11.9 %all-to-all-done.1.a_ref = bf16[8,64,256]{2,1,0:T(8,128)(2,1)S(1)} async-done(((bf16[8,64,256]{2,1,0:T(8,128)(2,1)}), bf16[8,64,256]{2,1,0:T(8,128)(2,1)S(1)}, u32[]{:S(2)}, u32[]{:S(2)}) %all-to-all-start.1) | async-done | bytes 262176 | tf_op jit(solution)/shard_map/all_to_all | solution.py:440
  146.5 0.0 copy-start.5
  146.5 0.7 copy-done.5
  147.2 9.0 %project.1 = (bf16[64,2048]{1,0:T(8,128)(2,1)}, bf16[16,160,128]{2,1,0:T(8,128)(2,1)}) custom-call(bf16[8,64,256]{2,1,0:T(8,128)(2,1)} %copy-done.5, bf16[2048,2048]{1,0:T(8,128)(2,1)} %w_ref.1, bf16[64,2048]{1,0:T(8,128)(2,1)} %res_ref.1, f32[1,2048]{1,0:T(1,128)} %bitcast.9, s32[64,2]{1,0:T(8,128)} %copy.19.route_ref, s32[2,64]{1,0:T(2,128)} %bitcast.7), custom_call_target="tpu_custom_call" | custom-call | tf_op jit(solution)/shard_map/project/pallas_call | solution.py:273
  156.2 15.1 %all_to_all.20.in_ref = bf16[16,160,128]{2,1,0:T(8,128)(2,1)} all-to-all(bf16[16,160,128]{2,1,0:T(8,128)(2,1)} %get-tuple-element.15), channel_id=1, replica_groups=mesh['sp'=16,'z'=8,'core'=2] {'sp'}, dimensions={0} | all-to-all | bytes 1310720 | tf_op jit(solution)/shard_map/all_to_all | solution.py:445
  171.3 0.0 all-gather.4.cloned.1.call-done.gate_ref
  171.3 0.0 all-gather.6.cloned.1.call-done.up_ref
  171.3 10.9 %hidden.1.hid_ref = bf16[160,2048]{1,0:T(8,128)(2,1)} custom-call(bf16[16,160,128]{2,1,0:T(8,128)(2,1)} %all_to_all.20.in_ref, bf16[16,2048,128]{2,1,0:T(8,128)(2,1)} %all-gather.4.cloned.1.call-done.gate_ref, bf16[16,2048,128]{2,1,0:T(8,128)(2,1)} %all-gather.6.cloned.1.call-done.up_ref), custom_call_target="tpu_custom_call" | custom-call | tf_op jit(solution)/shard_map/hidden/pallas_call | solution.py:313
  182.3 0.0 copy-start.7
  182.3 0.0 copy-start.8
  182.3 2.5 %all-gather.8.cloned.1.call-done.down_ref = bf16[16,128,2048]{2,1,0:T(8,128)(2,1)} async-done(((bf16[1,128,2048]{2,1,0:T(8,128)(2,1)}), bf16[16,128,2048]{2,1,0:T(8,128)(2,1)}) %all-gather.8.cloned.1.call-update) | async-done | bytes 8388624 | tf_op jit(solution)/shard_map/all_gather | solution.py:418
  184.8 8.9 %down.1 = bf16[16,160,128]{2,1,0:T(8,128)(2,1)} custom-call(bf16[160,2048]{1,0:T(8,128)(2,1)} %hidden.1.hid_ref, bf16[16,128,2048]{2,1,0:T(8,128)(2,1)} %all-gather.8.cloned.1.call-done.down_ref), custom_call_target="tpu_custom_call" | custom-call | tf_op jit(solution)/shard_map/down/pallas_call | solution.py:344
  193.7 4.5 %all-to-all-start.3 = ((bf16[16,160,128]{2,1,0:T(8,128)(2,1)}), bf16[16,160,128]{2,1,0:T(8,128)(2,1)S(1)}, u32[]{:S(2)}, u32[]{:S(2)}) async-start(bf16[16,160,128]{2,1,0:T(8,128)(2,1)} %down.1), calls=%async_computation.3 | async-start | bytes 1310720 | tf_op jit(solution)/shard_map/all_to_all | solution.py:448
  198.1 0.0 copy-done.7
  198.2 0.7 copy.21.score_ref
  198.9 0.0 copy-done.8
  198.9 0.7 copy.22.prob_ref
  199.6 10.8 %all-to-all-done.3.in_ref = bf16[16,160,128]{2,1,0:T(8,128)(2,1)S(1)} async-done(((bf16[16,160,128]{2,1,0:T(8,128)(2,1)}), bf16[16,160,128]{2,1,0:T(8,128)(2,1)S(1)}, u32[]{:S(2)}, u32[]{:S(2)}) %all-to-all-start.3) | async-done | bytes 655392 | tf_op jit(solution)/shard_map/all_to_all | solution.py:448
  210.4 0.0 copy-start.3
  210.4 0.8 copy-done.3
  211.2 2.8 %mix.1 = bf16[64,2048]{1,0:T(8,128)(2,1)} custom-call(bf16[16,160,128]{2,1,0:T(8,128)(2,1)} %copy-done.3, bf16[64,2048]{1,0:T(8,128)(2,1)} %get-tuple-element.16.upd_ref, s32[64,2]{1,0:T(8,128)} %copy.19.route_ref, s32[2,64]{1,0:T(2,128)} %bitcast.8, f32[64,2]{1,0:T(8,128)} %copy.21.score_ref, f32[64,1]{1,0:T(8,128)} %copy.22.prob_ref), custom_call_target="tpu_custom_call" | custom-call | tf_op jit(solution)/shard_map/mix/pallas_call | solution.py:387
  (2 shorter events, 0.0 us)
Async XLA Ops:
  6.5 164.8 %all-gather.4.cloned.1.call-start = ((), (), s32[]{:S(2)}) async-start(), calls=%async_computation.4 | async-start | bytes 8912896 | tf_op jit(solution)/shard_map/all_gather | solution.py:416
  7.3 164.1 %all-gather.6.cloned.1.call-start = ((), (), s32[]{:S(2)}) async-start(), calls=%async_computation.5 | async-start | bytes 8912896 | tf_op jit(solution)/shard_map/all_gather | solution.py:417
  8.0 176.7 %all-gather.8.cloned.1.call-start = ((), (), s32[]{:S(2)}) async-start(), calls=%async_computation.6 | async-start | bytes 8912896 | tf_op jit(solution)/shard_map/all_gather | solution.py:418
  9.3 79.7 %copy-start.2 = (s32[2]{0:T(128)S(1)}, s32[2]{0:T(128)}, u32[]{:S(2)}) copy-start(s32[2]{0:T(128)} %pad_add_fusion.where_ref) | copy-start | bytes 28
  15.4 11.2 %copy-start.1 = (bf16[1024,128]{1,0:T(8,128)(2,1)S(1)}, bf16[1024,128]{1,0:T(8,128)(2,1)}, u32[]{:S(2)}) copy-start(bf16[1024,128]{1,0:T(8,128)(2,1)} %get-tuple-element.11.own_ref) | copy-start | bytes 786436
  18.8 115.0 %copy-start.6 = (s32[64,2]{0,1:T(2,128)S(1)}, s32[64,2]{0,1:T(2,128)}, u32[]{:S(2)}) copy-start(s32[64,2]{0,1:T(2,128)} %param.22) | copy-start | bytes 1540
  18.8 70.2 %all-to-all-start = ((bf16[16,512,256]{2,1,0:T(8,128)(2,1)}), bf16[16,512,256]{2,1,0:T(8,128)(2,1)}, u32[]{:S(2)}, u32[]{:S(2)}) async-start(bf16[16,512,256]{2,1,0:T(8,128)(2,1)} %broadcast_in_dim.33), calls=%async_computation | async-start | bytes 8388608 | tf_op jit(solution)/shard_map/all_to_all | solution.py:435
  26.6 2.2 collective-permute-start
  116.2 1.1 copy-start
  117.3 4.3 %collective-permute-start.1 = (f32[2,8,64,256]{3,2,1,0:T(8,128)S(1)}, f32[2,8,64,256]{3,2,1,0:T(8,128)S(1)}, u32[]{:S(2)}, u32[]{:S(2)}) collective-permute-start(f32[2,8,64,256]{3,2,1,0:T(8,128)S(1)} %get-tuple-element.14), channel_id=1, source_target_pairs={{0,1},{1,0},{2,3},{3,2},{4,5},{5,4},{6,7},{7,6},{8,9},{9,8},{10,11... | collective-permute-start | bytes 3145736 | tf_op jit(solution)/shard_map/ppermute | solution.py:439
  121.5 1.0 copy-start.4
  125.7 20.8 %all-to-all-start.1 = ((bf16[8,64,256]{2,1,0:T(8,128)(2,1)}), bf16[8,64,256]{2,1,0:T(8,128)(2,1)S(1)}, u32[]{:S(2)}, u32[]{:S(2)}) async-start(bf16[8,64,256]{2,1,0:T(8,128)(2,1)} %merge.1), calls=%async_computation.1 | async-start | bytes 524288 | tf_op jit(solution)/shard_map/all_to_all | solution.py:440
  146.5 0.7 copy-start.5
  182.3 15.9 %copy-start.7 = (f32[64,2]{0,1:T(2,128)S(1)}, f32[64,2]{0,1:T(2,128)}, u32[]{:S(2)}) copy-start(f32[64,2]{0,1:T(2,128)} %param.23) | copy-start | bytes 1540
  182.3 16.6 %copy-start.8 = (f32[64]{0:T(128)S(1)}, f32[64]{0:T(128)}, u32[]{:S(2)}) copy-start(f32[64]{0:T(128)} %param.24) | copy-start | bytes 772
  193.7 16.7 %all-to-all-start.3 = ((bf16[16,160,128]{2,1,0:T(8,128)(2,1)}), bf16[16,160,128]{2,1,0:T(8,128)(2,1)S(1)}, u32[]{:S(2)}, u32[]{:S(2)}) async-start(bf16[16,160,128]{2,1,0:T(8,128)(2,1)} %down.1), calls=%async_computation.3 | async-start | bytes 1310720 | tf_op jit(solution)/shard_map/all_to_all | solution.py:448
  210.4 0.8 copy-start.3
Sparse Core Ops, SparseCore 0:
  9.2 60.0 all-gather.3
  71.1 54.3 all-gather.5
  127.3 57.3 all-gather.7
